TPU v7x, 256 devices: a whole 4x4x8 slice. The times are simulated.
256 devices in a mesh: sp: 16 (over y, x), tp: 16 (over z, core).
Axes of the slice: x: 4, y: 4, z: 8, core: 2. Of those that a mesh axis runs over, the one named last changes fastest.
Arguments:
- residual: bfloat16 [8192, 2048], P(('sp', 'tp')), may hold values from -6 to 6
- queries: bfloat16 [8192, 4096], P('sp', 'tp'), may hold values from -6 to 6
- keys: bfloat16 [8192, 4096], P('sp', 'tp'), may hold values from -6 to 6
- values: bfloat16 [8192, 4096], P('sp', 'tp'), may hold values from -6 to 6
- in_gate: float32 [16, 8192], P('tp', 'sp'), may hold values from -5 to 130
- forget_gate: float32 [16, 8192], P('tp', 'sp'), may hold values from 0 to 16
- doc_ids: int32 [8192], P('sp'), may hold values from 0 to 7, never falling along the last dimension, each value on 1 to 4096 neighbouring positions
- head_gain: float32 [4096], P('tp'), may hold values from 0.1 to 1.9
- out_weight: bfloat16 [4096, 2048], P('tp'), may hold values from -0.09375 to 0.09375
- norm_gain: float32 [2048], replicated, may hold values from 0.1 to 1.9
- route_ids: int32 [8192, 2], P(('sp', 'tp')), may hold values from 0 to 15, all different within a row; in each aligned block of 32 rows (0 to 31, 32 to 63, ...) at most 5 rows name the same one
- route_weights: float32 [8192, 2], P(('sp', 'tp')), may hold values from 0.2 to 1
- gate_proj: bfloat16 [16, 2048, 4096], P('sp', None, 'tp'), may hold values from -0.125 to 0.125
- up_proj: bfloat16 [16, 2048, 4096], P('sp', None, 'tp'), may hold values from -0.125 to 0.125
- down_proj: bfloat16 [16, 4096, 2048], P('sp', 'tp'), may hold values from -0.09375 to 0.09375
Outputs:
- mixed: bfloat16 [8192, 2048], P(('sp', 'tp'))
Inputs may be any that keep to these rules, and one draw needn't show every extreme that they name: `route_ids`: each row names 2 different experts. In each aligned block of 32 rows (the rows of one device) no expert is named by more than 5 rows, and in some blocks one expert by exactly 5. `doc_ids`: numbers never fall along the sequence; no document covers more than half of the 8192 positions, and one covers exactly half.
All inputs are finite; a program needn't handle non-finite values.
Results may differ from a plain program's by a relative error of at most 0.018.
Values may be sent and summed in bfloat16 or wider, within the bound.
A program may use at most 64 MiB of HBM per device.

v0:
```python
import math
import jax
import jax.numpy as jnp
from jax import lax
from jax.sharding import Mesh
from jax.sharding import PartitionSpec as P

SP = ("sp_0", "sp_1")
SP_TP = ("sp_0", "sp_1", "tp")
MASKED = -1e30
EPSILON = 1e-06


def neutral_like(value, identity):
    return jax.tree.map(
        lambda a, e: jnp.broadcast_to(jnp.asarray(e, a.dtype), a.shape), value, identity
    )


def carried_in(value, axes, combine, identity):
    before = start = neutral_like(value, identity)
    running = value
    for axis in reversed(axes):
        peers, index = (lax.axis_size(axis), lax.axis_index(axis))
        pieces = jax.tree.map(lambda part: lax.all_gather(part, axis), running)
        inside, running = (start, start)
        for k in range(peers):
            passed = k < index
            running = combine(running, jax.tree.map(lambda part: part[k], pieces))
            inside = jax.tree.map(lambda new, old: jnp.where(passed, new, old), running, inside)
        before = combine(inside, before)
    return before


def block_step(state, pieces):
    memory, normalizer, max_level, carry_doc = state
    q_block, k_block, v_block, in_block, forget_block, doc_block = pieces
    scaling = q_block.shape[1] ** (-0.5)
    cum_forget = jnp.cumsum(forget_block)
    positions = jnp.arange(q_block.shape[0])
    permitted_mask = (positions[:, None] >= positions[None, :]) & (
        doc_block[:, None] == doc_block[None, :]
    )
    log_weights = jnp.where(
        permitted_mask, cum_forget[:, None] - cum_forget[None, :] + in_block[None, :], MASKED
    )
    carried = jnp.where(doc_block == carry_doc, cum_forget + max_level, MASKED)
    row_max = jnp.maximum(carried, jnp.max(log_weights, axis=1))
    scores = jnp.dot(q_block, k_block.T, preferred_element_type=jnp.float32) * scaling
    weighted = scores * jnp.exp(log_weights - row_max[:, None])
    carry_weight = jnp.exp(carried - row_max)
    query_scaled = q_block.astype(jnp.float32) * scaling
    key_full = k_block.astype(jnp.float32)
    value_full = v_block.astype(jnp.float32)
    readout_numerator = jnp.dot(weighted, value_full, precision=lax.Precision.HIGHEST)
    readout_numerator = readout_numerator + carry_weight[:, None] * jnp.dot(
        query_scaled, memory.T, precision=lax.Precision.HIGHEST
    )
    denominator = jnp.sum(weighted, axis=1) + carry_weight * jnp.dot(
        query_scaled, normalizer, precision=lax.Precision.HIGHEST
    )
    last_doc = doc_block[-1]
    forget_total = cum_forget[-1]
    log_end = jnp.where(doc_block == last_doc, forget_total - cum_forget + in_block, MASKED)
    carry_log = jnp.where(carry_doc == last_doc, forget_total + max_level, MASKED)
    new_max = jnp.maximum(carry_log, jnp.max(log_end))
    end_weight = jnp.exp(log_end - new_max)
    kept_share = jnp.exp(carry_log - new_max)
    new_memory = kept_share * memory + jnp.dot(
        (value_full * end_weight[:, None]).T, key_full, precision=lax.Precision.HIGHEST
    )
    new_normalizer = kept_share * normalizer + jnp.dot(
        end_weight, key_full, precision=lax.Precision.HIGHEST
    )
    return (
        (new_memory, new_normalizer, new_max, last_doc),
        (readout_numerator, denominator, row_max),
    )


def run_blocks(
    queries_in,
    keys_in,
    incoming_vectors,
    in_gates,
    log_forget,
    doc_row,
    memory,
    normalizer,
    max_level,
    carry_doc,
):
    extent = queries_in.shape[0]
    block_size = math.gcd(extent, 256)
    blocks = extent // block_size

    def to_blocks(tensor):
        return tensor.reshape((blocks, block_size) + tensor.shape[1:])

    pieces = tuple(
        (
            to_blocks(tensor)
            for tensor in (queries_in, keys_in, incoming_vectors, in_gates, log_forget, doc_row)
        )
    )
    final_state, outputs = lax.scan(block_step, (memory, normalizer, max_level, carry_doc), pieces)
    readout_numerator, denominator, row_max = outputs
    return (
        readout_numerator.reshape(extent, -1),
        denominator.reshape(extent),
        row_max.reshape(extent),
        final_state,
    )


def combine_states(earlier, later):
    memory_a, normal_a, level_a, forget_a, first_a, last_a = earlier
    memory_b, normal_b, level_b, forget_b, first_b, last_b = later
    joined = (last_a == first_b) | (last_a < 0) | (first_b < 0)
    passed = forget_b + jnp.where(joined, 0.0, MASKED)
    new_level = jnp.maximum(passed + level_a, level_b)
    share_a = jnp.exp(passed + level_a - new_level)
    fraction_second = jnp.exp(level_b - new_level)
    new_memory = share_a[:, None, None] * memory_a + fraction_second[:, None, None] * memory_b
    new_normal = share_a[:, None] * normal_a + fraction_second[:, None] * normal_b
    first_doc = jnp.where(first_a < 0, first_b, first_a)
    last_doc = jnp.where(last_b < 0, last_a, last_b)
    return (new_memory, new_normal, new_level, forget_a + passed, first_doc, last_doc)


def on_device(
    residual,
    queries,
    keys,
    values,
    in_gate,
    forget_gate,
    doc_ids,
    head_gain,
    out_weight,
    norm_gain,
    route_ids,
    route_weights,
    gate_proj,
    up_proj,
    down_proj,
):
    extent, local_width = queries.shape
    heads_here = in_gate.shape[0]
    head_size = local_width // heads_here

    def by_head(tensor):
        return tensor.reshape(extent, heads_here, head_size).transpose(1, 0, 2)

    query_heads = by_head(queries)
    key_heads = by_head(keys)
    value_heads = by_head(values)
    log_forget = jax.nn.log_sigmoid(forget_gate)
    cum_forget = jnp.cumsum(log_forget, axis=1)
    first_doc = doc_ids[0]
    last_doc = doc_ids[-1]
    run_heads = jax.vmap(run_blocks, in_axes=(0, 0, 0, 0, 0, None, 0, 0, 0, None))
    forget_total = jnp.where(first_doc == last_doc, cum_forget[:, -1], MASKED)
    doc_first = first_doc.astype(jnp.float32).reshape(1)
    doc_last = last_doc.astype(jnp.float32).reshape(1)
    empty_memory = jnp.zeros((heads_here, head_size, head_size), jnp.float32)
    empty_normal = jnp.zeros((heads_here, head_size), jnp.float32)
    empty_level = jnp.full((heads_here,), MASKED, jnp.float32)
    identity = (
        empty_memory,
        empty_normal,
        empty_level,
        jnp.zeros((heads_here,), jnp.float32),
        jnp.full((1,), -1.0, jnp.float32),
        jnp.full((1,), -1.0, jnp.float32),
    )
    readout_numerator, denominator, row_max, final_state = run_heads(
        query_heads,
        key_heads,
        value_heads,
        in_gate,
        log_forget,
        doc_ids,
        empty_memory,
        empty_normal,
        empty_level,
        first_doc,
    )
    local_state = (
        final_state[0],
        final_state[1],
        final_state[2],
        forget_total,
        doc_first,
        doc_last,
    )
    incoming = carried_in(local_state, SP, combine_states, identity)
    linked = incoming[5][0] == doc_first[0]
    in_level = jnp.where(linked, incoming[2], MASKED)
    carried = jnp.where(doc_ids[None, :] == first_doc, cum_forget + in_level[:, None], MASKED)
    new_max = jnp.maximum(row_max, carried)
    own_share = jnp.exp(row_max - new_max)
    far_share = jnp.exp(carried - new_max)
    query_scaled = query_heads.astype(jnp.float32) * head_size ** (-0.5)
    readout_numerator = own_share[..., None] * readout_numerator + far_share[
        ..., None
    ] * jnp.einsum("htd,hvd->htv", query_scaled, incoming[0], precision=lax.Precision.HIGHEST)
    denominator = own_share * denominator + far_share * jnp.einsum(
        "htd,hd->ht", query_scaled, incoming[1], precision=lax.Precision.HIGHEST
    )
    mixed_heads = (
        readout_numerator / jnp.maximum(jnp.abs(denominator), jnp.exp(-new_max))[..., None]
    )
    normed_heads = mixed_heads * lax.rsqrt(
        jnp.mean(mixed_heads * mixed_heads, axis=-1, keepdims=True) + EPSILON
    )
    normed_heads = normed_heads * head_gain.reshape(heads_here, 1, head_size)
    head_rows = normed_heads.transpose(1, 0, 2).reshape(extent, local_width).astype(jnp.bfloat16)
    rows_here, model_width = residual.shape
    update = lax.psum_scatter(
        jnp.dot(head_rows, out_weight, preferred_element_type=jnp.float32).astype(jnp.bfloat16),
        "tp",
        scatter_dimension=0,
        tiled=True,
    ).astype(jnp.float32)
    stream = residual.astype(jnp.float32) + update
    normed = (
        stream * lax.rsqrt(jnp.mean(stream * stream, axis=-1, keepdims=True) + EPSILON) * norm_gain
    )
    normed = normed.astype(jnp.bfloat16)
    experts_all = gate_proj.shape[0] * lax.axis_size(SP)
    top_count = route_ids.shape[1]
    capacity = max(2, rows_here * top_count * 5 // (4 * experts_all))
    flat_ids = route_ids.reshape(-1)
    onehot = (flat_ids[:, None] == jnp.arange(experts_all, dtype=jnp.int32)[None, :]).astype(
        jnp.int32
    )
    earlier = jnp.cumsum(onehot, axis=0) - onehot
    slot_rank = jnp.sum(earlier * onehot, axis=1)
    slot_index = flat_ids * capacity + slot_rank
    placing = (
        slot_index[None, :] == jnp.arange(experts_all * capacity, dtype=jnp.int32)[:, None]
    ).astype(jnp.bfloat16)
    copies = jnp.repeat(normed, top_count, axis=0)
    outgoing = jnp.dot(placing, copies, preferred_element_type=jnp.float32).astype(jnp.bfloat16)
    outgoing = outgoing.reshape(experts_all, capacity, model_width)
    arrived = lax.all_to_all(outgoing, SP, split_axis=0, concat_axis=0, tiled=True).reshape(
        -1, model_width
    )
    piece = lax.all_gather(arrived, "tp", axis=0, tiled=True)
    gate_part = jnp.dot(piece, gate_proj[0], preferred_element_type=jnp.float32)
    up_part = jnp.dot(piece, up_proj[0], preferred_element_type=jnp.float32)
    hidden = (jax.nn.silu(gate_part) * up_part).astype(jnp.bfloat16)
    expert_sum = lax.psum_scatter(
        jnp.dot(hidden, down_proj[0], preferred_element_type=jnp.float32).astype(jnp.bfloat16),
        "tp",
        scatter_dimension=0,
        tiled=True,
    )
    expert_out = expert_sum.reshape(experts_all, capacity, model_width)
    returned = lax.all_to_all(expert_out, SP, split_axis=0, concat_axis=0, tiled=True)
    picked = jnp.take(returned.reshape(-1, model_width), slot_index, axis=0)
    picked = picked.reshape(rows_here, top_count, model_width)
    expert_mix = jnp.sum(route_weights[..., None] * picked.astype(jnp.float32), axis=1)
    return (stream + expert_mix).astype(jnp.bfloat16)


def solution(mesh):
    finer = Mesh(mesh.devices.reshape(4, 4, mesh.shape["tp"]), ("sp_0", "sp_1", "tp"))
    in_specs = (
        P(SP_TP, None),
        P(SP, "tp"),
        P(SP, "tp"),
        P(SP, "tp"),
        P("tp", SP),
        P("tp", SP),
        P(SP),
        P("tp"),
        P("tp", None),
        P(),
        P(SP_TP, None),
        P(SP_TP, None),
        P(SP, None, "tp"),
        P(SP, None, "tp"),
        P(SP, "tp", None),
    )
    out_specs = P(SP_TP, None)
    return jax.shard_map(
        on_device, mesh=finer, in_specs=in_specs, out_specs=out_specs, check_vma=False
    )
```

profile of v0, /device:TPU:2, one launch (start us, length us, event | category | flops | bytes accessed | tf_op | source)
XLA Modules:
  0.0 372.2 jit_solution(4518122679349654062)
XLA Ops:
  10.0 25.1 %while.23 = (s32[]{:T(128)}, f32[1,256,256]{2,1,0:T(8,128)S(1)}, f32[1,256]{1,0:T(1,128)S(1)}, f32[1]{0:T(128)}, s32[]{:T(128)}, /*index=5*/f32[2,1,256,256]{3,2...) while((s32[]{:T(128)}, f32[1,256,256]{2,1,0:T(8,128)S(1)}, ...), condition=%wide.region_6.7_spmd.clone, body=%wide.region_0.6_spmd.clone.sunk | while | flops 641046528 | bytes 6349332 | solution.py:106
  15.7 1.9 fusion.223
  28.2 1.9 fusion.223
  45.2 10.0 %all-reduce.8 = (f32[4]{0:T(128)S(1)}, f32[4]{0:T(128)S(1)}, f32[4]{0:T(128)S(1)}, f32[4]{0:T(128)S(1)}) all-reduce(f32[4]{0:T(128)S(1)} %dynamic-update-slice, f32[4]{0:T(128)S(1)} %fusion.156, f32[4]{0:T(128)S(1)} %dynamic-update-slice.3, f32[4]{0:T(128)S(1)} %dynamic-update-slice.6), channel_id=1, replica_groups=mesh['sp_0'=4,'sp_1'=4,'tp'=16] {'sp_1'}, use_global_device_ids=true, to_apply=%add | all-reduce | flops 16 | bytes 128
  55.9 2.6 fusion.152
  72.3 2.0 fusion.70
  75.1 1.9 fusion.188
  80.3 1.4 dynamic-update-slice.5
  81.8 1.4 dynamic-update-slice.1
  83.2 9.3 %all-reduce.9 = (f32[4]{0:T(128)S(1)}, f32[4]{0:T(128)S(1)}, f32[4]{0:T(128)S(1)}, f32[4]{0:T(128)S(1)}) all-reduce(f32[4]{0:T(128)S(1)} %dynamic-update-slice.1, f32[4]{0:T(128)S(1)} %dynamic-update-slice.4, f32[4]{0:T(128)S(1)} %dynamic-update-slice.5, f32[4]{0:T(128)S(1)} %dynamic-update-slice.7), channel_id=2, replica_groups=mesh['sp_0'=4,'sp_1'=4,'tp'=16] {'sp_0'}, use_global_device_ids=true, to_apply=%add.1 | all-reduce | flops 16 | bytes 128
  121.3 9.6 %all-gather.8 = f32[4,1,256]{2,1,0:T(1,128)S(1)} all-gather(f32[1,1,256]{2,1,0:T(1,128)S(1)} %bitcast.322), channel_id=9, replica_groups=mesh['sp_0'=4,'sp_1'=4,'tp'=16] {'sp_1'}, dimensions={0}, use_global_device_ids=true | all-gather | bytes 5120 | tf_op jit(solution)/shard_map/all_gather | solution.py:25
  130.9 7.0 %all_gather.84 = f32[4,1,256]{2,1,0:T(1,128)S(1)} all-gather(f32[1,1,256]{2,1,0:T(1,128)S(1)} %get-tuple-element.176), channel_id=1, replica_groups=mesh['sp_0'=4,'sp_1'=4,'tp'=16] {'sp_0'}, dimensions={0}, use_global_device_ids=true | all-gather | bytes 5120 | tf_op jit(solution)/shard_map/all_gather | solution.py:25
  139.3 2.6 multiply_reduce_fusion.1
  141.9 2.2 convolution_convert_fusion.1
  144.7 59.9 %reduce-scatter.3.cloned.1.call-done = bf16[32,2048]{1,0:T(8,128)(2,1)} async-done(((bf16[512,2048]{1,0:T(8,128)(2,1)}), bf16[32,2048]{1,0:T(8,128)(2,1)}) %reduce-scatter.3.cloned.1.call-update) | async-done | bytes 131088 | tf_op jit(solution)/shard_map/reduce_scatter | solution.py:220
  207.4 15.9 %all_to_all.10 = bf16[16,5,2048]{2,1,0:T(8,128)(2,1)S(1)} all-to-all(bf16[16,5,2048]{2,1,0:T(8,128)(2,1)S(1)} %reshape.898), channel_id=1, replica_groups=mesh['sp_0'=4,'sp_1'=4,'tp'=16] {'sp_0','sp_1'}, dimensions={0} | all-to-all | bytes 655360 | tf_op jit(solution)/shard_map/all_to_all | solution.py:247
  224.4 40.1 %all-gather.15.cloned.1.call-done = bf16[1280,2048]{1,0:T(8,128)(2,1)} async-done(((bf16[80,2048]{1,0:T(8,128)(2,1)}), bf16[1280,2048]{1,0:T(8,128)(2,1)}) %all-gather.15.cloned.1.call-update) | async-done | bytes 5242896 | tf_op jit(solution)/shard_map/all_gather | solution.py:250
  264.5 5.1 %fusion.56 = f32[1280,256]{1,0:T(8,128)} fusion(bf16[1280,2048]{1,0:T(8,128)(2,1)} %all-gather.15.cloned.1.call-done, bf16[1,2048,256]{2,1,0:T(8,128)(2,1)S(1)} %copy-done.14), kind=kOutput, calls=%fused_computation.85 | convolution fusion | flops 1342177280 | bytes 7602176 | tf_op jit(solution)/shard_map/dot_general | solution.py:251
  269.6 10.6 %convolution_convert_fusion = bf16[1280,2048]{1,0:T(8,128)(2,1)} fusion(bf16[1280,2048]{1,0:T(8,128)(2,1)} %all-gather.15.cloned.1.call-done, f32[1280,256]{1,0:T(8,128)} %fusion.56, bf16[1,256,2048]{2,1,0:T(8,128)(2,1)S(1)} %copy-done, bf16[1,2048,256]{2,1,0:T(8,128)(2,1)S(1)} %copy-done.15), kind=kOutput, calls=%fused_computation.75 | convolution fusion | flops 2688942080 | bytes 13893632 | tf_op jit(solution)/shard_map/dot_general | solution.py:255
  280.9 63.2 %reduce-scatter.5.cloned.1.call-done = bf16[80,2048]{1,0:T(8,128)(2,1)} async-done(((bf16[1280,2048]{1,0:T(8,128)(2,1)}), bf16[80,2048]{1,0:T(8,128)(2,1)}) %reduce-scatter.5.cloned.1.call-update) | async-done | bytes 327696 | tf_op jit(solution)/shard_map/reduce_scatter | solution.py:254
  344.2 1.9 reshape.900
  346.1 7.3 %all-to-all-start.1 = ((bf16[16,5,2048]{2,1,0:T(8,128)(2,1)}), bf16[16,5,2048]{2,1,0:T(8,128)(2,1)S(1)}, u32[]{:S(2)}, u32[]{:S(2)}) async-start(bf16[16,5,2048]{2,1,0:T(8,128)(2,1)} %reshape.900), calls=%async_computation.3 | async-start | bytes 1048576 | tf_op jit(solution)/shard_map/all_to_all | solution.py:261
  353.4 8.7 %all-to-all-done.1 = bf16[16,5,2048]{2,1,0:T(8,128)(2,1)S(1)} async-done(((bf16[16,5,2048]{2,1,0:T(8,128)(2,1)}), bf16[16,5,2048]{2,1,0:T(8,128)(2,1)S(1)}, u32[]{:S(2)}, u32[]{:S(2)}) %all-to-all-start.1) | async-done | bytes 327712 | tf_op jit(solution)/shard_map/all_to_all | solution.py:261
  363.2 1.8 multiply_reduce_fusion
  (169 shorter events, 42.9 us)
Async XLA Ops:
  6.5 263.0 %copy-start = (bf16[1,256,2048]{2,1,0:T(8,128)(2,1)S(1)}, bf16[1,256,2048]{2,1,0:T(8,128)(2,1)}, u32[]{:S(2)}) copy-start(bf16[1,256,2048]{2,1,0:T(8,128)(2,1)} %param.31) | copy-start | bytes 3145732
  6.5 65.7 %all-gather.17.cloned.1.call-start = ((), (), s32[]{:S(2)}) async-start(), calls=%async_computation.8 | async-start | bytes 1310720 | tf_op jit(solution)/shard_map/all_gather | solution.py:25
  10.0 31.6 %copy-start.17 = (u32[256]{0:T(256)S(1)}, u32[256]{0:T(256)}, u32[]{:S(2)}) copy-start(u32[256]{0:T(256)} %constant.127) | copy-start | bytes 3076
  10.0 64.3 %copy-start.16 = (u32[256]{0:T(256)S(1)}, u32[256]{0:T(256)}, u32[]{:S(2)}) copy-start(u32[256]{0:T(256)} %constant.132) | copy-start | bytes 3076
  10.1 10.8 %copy-start.4 = (bf16[2,1,256,256]{3,2,1,0:T(8,128)(2,1)S(1)}, bf16[2,1,256,256]{3,2,1,0:T(8,128)(2,1)}, u32[]{:S(2)}) copy-start(bf16[2,1,256,256]{3,2,1,0:T(8,128)(2,1)} %get-tuple-element.388) | copy-start | bytes 786436 | tf_op jit(solution)/shard_map/vmap()/while
  10.1 10.8 %copy-start.5 = (bf16[2,1,256,256]{3,2,1,0:T(8,128)(2,1)S(1)}, bf16[2,1,256,256]{3,2,1,0:T(8,128)(2,1)}, u32[]{:S(2)}) copy-start(bf16[2,1,256,256]{3,2,1,0:T(8,128)(2,1)} %get-tuple-element.387) | copy-start | bytes 786436 | tf_op jit(solution)/shard_map/vmap()/while
  10.1 11.3 %copy-start.2 = (bf16[2,1,256,256]{3,2,1,0:T(8,128)(2,1)S(1)}, bf16[2,1,256,256]{3,2,1,0:T(8,128)(2,1)}, u32[]{:S(2)}) copy-start(bf16[2,1,256,256]{3,2,1,0:T(8,128)(2,1)} %get-tuple-element.389) | copy-start | bytes 786436 | tf_op jit(solution)/shard_map/vmap()/while
  22.6 10.8 %copy-start.4 = (bf16[2,1,256,256]{3,2,1,0:T(8,128)(2,1)S(1)}, bf16[2,1,256,256]{3,2,1,0:T(8,128)(2,1)}, u32[]{:S(2)}) copy-start(bf16[2,1,256,256]{3,2,1,0:T(8,128)(2,1)} %get-tuple-element.388) | copy-start | bytes 786436 | tf_op jit(solution)/shard_map/vmap()/while
  22.6 10.8 %copy-start.5 = (bf16[2,1,256,256]{3,2,1,0:T(8,128)(2,1)S(1)}, bf16[2,1,256,256]{3,2,1,0:T(8,128)(2,1)}, u32[]{:S(2)}) copy-start(bf16[2,1,256,256]{3,2,1,0:T(8,128)(2,1)} %get-tuple-element.387) | copy-start | bytes 786436 | tf_op jit(solution)/shard_map/vmap()/while
  22.6 11.3 %copy-start.2 = (bf16[2,1,256,256]{3,2,1,0:T(8,128)(2,1)S(1)}, bf16[2,1,256,256]{3,2,1,0:T(8,128)(2,1)}, u32[]{:S(2)}) copy-start(bf16[2,1,256,256]{3,2,1,0:T(8,128)(2,1)} %get-tuple-element.389) | copy-start | bytes 786436 | tf_op jit(solution)/shard_map/vmap()/while
  35.1 102.7 %copy-start.9 = (s32[512]{0:T(512)S(1)}, s32[512]{0:T(512)}, u32[]{:S(2)}) copy-start(s32[512]{0:T(512)} %param.23) | copy-start | bytes 6148
  35.2 103.5 %copy-start.3 = (bf16[2,1,256,256]{3,2,1,0:T(8,128)(2,1)S(1)}, bf16[2,1,256,256]{3,2,1,0:T(8,128)(2,1)}, u32[]{:S(2)}) copy-start(bf16[2,1,256,256]{3,2,1,0:T(8,128)(2,1)} %get-tuple-element.404) | copy-start | bytes 786436
  35.9 103.4 %all-gather.13.cloned.1.call-start = ((), (), s32[]{:S(2)}) async-start(), calls=%async_computation.4 | async-start | bytes 1310720 | tf_op jit(solution)/shard_map/all_gather | solution.py:25
  74.3 130.3 %reduce-scatter.3.cloned.1.call-start = ((), (), s32[]{:S(2)}) async-start(), calls=%async_computation.5 | async-start | bytes 2228224 | tf_op jit(solution)/shard_map/reduce_scatter | solution.py:220
  139.3 2.6 copy-start.8
  139.3 2.6 copy-start.13
  141.9 62.7 %copy-start.6 = (bf16[32,2048]{1,0:T(8,128)(2,1)S(1)}, bf16[32,2048]{1,0:T(8,128)(2,1)}, u32[]{:S(2)}) copy-start(bf16[32,2048]{1,0:T(8,128)(2,1)} %param.17) | copy-start | bytes 393220
  144.1 61.6 %copy-start.11 = (f32[2048]{0:T(1024)S(1)}, f32[2048]{0:T(1024)}, u32[]{:S(2)}) copy-start(f32[2048]{0:T(1024)} %param.26) | copy-start | bytes 24580
  144.1 120.3 %all-gather.15.cloned.1.call-start = ((), (), s32[]{:S(2)}) async-start(), calls=%async_computation.6 | async-start | bytes 5570560 | tf_op jit(solution)/shard_map/all_gather | solution.py:250
  206.9 57.6 %copy-start.14 = (bf16[1,2048,256]{2,1,0:T(8,128)(2,1)S(1)}, bf16[1,2048,256]{2,1,0:T(8,128)(2,1)}, u32[]{:S(2)}) copy-start(bf16[1,2048,256]{2,1,0:T(8,128)(2,1)} %param.29) | copy-start | bytes 3145732
  224.1 45.4 %copy-start.15 = (bf16[1,2048,256]{2,1,0:T(8,128)(2,1)S(1)}, bf16[1,2048,256]{2,1,0:T(8,128)(2,1)}, u32[]{:S(2)}) copy-start(bf16[1,2048,256]{2,1,0:T(8,128)(2,1)} %param.30) | copy-start | bytes 3145732
  224.2 120.0 %reduce-scatter.5.cloned.1.call-start = ((), (), s32[]{:S(2)}) async-start(), calls=%async_computation.7 | async-start | bytes 5570560 | tf_op jit(solution)/shard_map/reduce_scatter | solution.py:254
  346.1 16.1 %all-to-all-start.1 = ((bf16[16,5,2048]{2,1,0:T(8,128)(2,1)}), bf16[16,5,2048]{2,1,0:T(8,128)(2,1)S(1)}, u32[]{:S(2)}, u32[]{:S(2)}) async-start(bf16[16,5,2048]{2,1,0:T(8,128)(2,1)} %reshape.900), calls=%async_computation.3 | async-start | bytes 1048576 | tf_op jit(solution)/shard_map/all_to_all | solution.py:261
  353.4 11.6 %copy-start.7 = (bf16[32,2048]{1,0:T(8,128)(2,1)S(1)}, bf16[32,2048]{1,0:T(8,128)(2,1)}, u32[]{:S(2)}) copy-start(bf16[32,2048]{1,0:T(8,128)(2,1)} %reduce-scatter.3.cloned.1.call-done) | copy-start | bytes 393220
  (3 other events, 3.6 us)
Sparse Core Ops, SparseCore 0:
  36.0 28.4 all-gather.16
  74.5 28.0 all-gather.12
  144.2 60.3 reduce-scatter.2
  224.3 40.1 all-gather.14
  280.3 63.8 reduce-scatter.4
where the time goes:
time: 374 us; the launch traced here: 372 us
  waiting for transfers between devices  172 us (46%)
  between operations  55.8 us (15%)
  blocking collectives  51.8 us (14%)
  matrix products  30.8 us (8%)
  local copies, waits for them, and re-layouts  25.3 us (7%)
  other arithmetic  23.4 us (6%)
  starting transfers between devices  7.62 us (2%)
  loops' own time  5.4 us (1%)
    reduce_scatter x1, waiting for transfers between devices, on_device(): lax.psum_scatter(jnp.dot(hidden, down_proj[0], preferred_element_type=jnp...  63.2 us
    reduce_scatter x1, waiting for transfers between devices, on_device(): lax.psum_scatter(jnp.dot(head_rows, out_weight, preferred_element_type=jn...  59.9 us
    all_gather x1, waiting for transfers between devices, on_device(): piece = lax.all_gather(arrived, 'tp', axis=0, tiled=True)  40.1 us
    unnamed x2, blocking collectives  19.3 us
    all_gather x2, blocking collectives, carried_in(): pieces = jax.tree.map(lambda part: lax.all_gather(part, axis), running)  16.6 us
    all_to_all x1, blocking collectives, on_device(): lax.all_to_all(outgoing, SP, split_axis=0, concat_axis=0, tiled=True)  15.9 us
    dot_general x1, matrix products, on_device(): jnp.dot(hidden, down_proj[0], preferred_element_type=jnp.float32)  10.6 us
    unnamed x49, local copies, waits for them, and re-layouts  9.59 us
  transfers between devices with their start and end apart: 6, of which 4 were waited for; matrix products, arithmetic and copies ran while one was open for 7% of the time, Pallas kernels for 0%

commit v1 on v0

--- a/solution.py
+++ b/solution.py
@@ -9,6 +9,13 @@
 SP_TP = ("sp_0", "sp_1", "tp")
 MASKED = -1e30
 EPSILON = 1e-06
+
+
+def read_cards(inputs):
+    outcome_arr = jnp.stack([inputs for _ in range(lax.axis_size("tp"))], 0)
+    mid_arr = lax.all_to_all(outcome_arr, axis_name="tp", split_axis=0, concat_axis=0)
+    x_next = jnp.concatenate(mid_arr, 0)
+    return x_next
 
 
 def neutral_like(value, identity):
@@ -247,7 +254,7 @@
     arrived = lax.all_to_all(outgoing, SP, split_axis=0, concat_axis=0, tiled=True).reshape(
         -1, model_width
     )
-    piece = lax.all_gather(arrived, "tp", axis=0, tiled=True)
+    piece = read_cards(arrived)
     gate_part = jnp.dot(piece, gate_proj[0], preferred_element_type=jnp.float32)
     up_part = jnp.dot(piece, up_proj[0], preferred_element_type=jnp.float32)
     hidden = (jax.nn.silu(gate_part) * up_part).astype(jnp.bfloat16)

time: 374 us -> 453 us (1.21)
  blocking collectives: 51.8 us -> 174 us
  waiting for transfers between devices: 172 us -> 129 us
    all_to_all x0 -> x1, blocking collectives: none -> 123 us  [read_cards(): lax.all_to_all(outcome_arr, axis_name='tp', split_axis=0, concat_axis=0)]
    all_gather x1 -> x0, waiting for transfers between devices: 40.1 us -> none  [on_device(): piece = lax.all_gather(arrived, 'tp', axis=0, tiled=True)]
    unnamed x49 -> x51, local copies, waits for them, and re-layouts: 9.59 us -> 11.5 us
  transfers between devices with their start and end apart: 6 -> 5, of which waited for: 4 -> 3; matrix products, arithmetic and copies ran while one was open for 7% -> 5% of each run, Pallas kernels for 0% -> 0%
where the time goes in v1:
time: 453 us; the launch traced here: 452 us
  blocking collectives  174 us (38%)
  waiting for transfers between devices  129 us (28%)
  between operations  56.9 us (13%)
  matrix products  28.3 us (6%)
  local copies, waits for them, and re-layouts  27.2 us (6%)
  other arithmetic  23.3 us (5%)
  starting transfers between devices  7.39 us (2%)
  loops' own time  5.15 us (1%)
    all_to_all x1, blocking collectives, read_cards(): lax.all_to_all(outcome_arr, axis_name='tp', split_axis=0, concat_axis=0)  123 us
    reduce_scatter x1, waiting for transfers between devices, on_device(): lax.psum_scatter(jnp.dot(hidden, down_proj[0], preferred_element_type=jnp...  60.4 us
    reduce_scatter x1, waiting for transfers between devices, on_device(): lax.psum_scatter(jnp.dot(head_rows, out_weight, preferred_element_type=jn...  59.8 us
    unnamed x2, blocking collectives  19.5 us
    all_gather x2, blocking collectives, carried_in(): pieces = jax.tree.map(lambda part: lax.all_gather(part, axis), running)  16.5 us
    all_to_all x1, blocking collectives, on_device(): lax.all_to_all(outgoing, SP, split_axis=0, concat_axis=0, tiled=True)  15.6 us
    unnamed x51, local copies, waits for them, and re-layouts  11.5 us
    dot_general x1, matrix products, on_device(): jnp.dot(hidden, down_proj[0], preferred_element_type=jnp.float32)  10.6 us
  transfers between devices with their start and end apart: 5, of which 3 were waited for; matrix products, arithmetic and copies ran while one was open for 5% of the time, Pallas kernels for 0%

profile of v1, /device:TPU:2, one launch (start us, length us, event | category | flops | bytes accessed | tf_op | source)
XLA Modules:
  0.0 451.5 jit_solution(17857413104721283777)
XLA Ops:
  6.5 1.4 fusion.182
  10.1 24.6 %while.23 = (s32[]{:T(128)}, f32[1,256,256]{2,1,0:T(8,128)S(1)}, f32[1,256]{1,0:T(1,128)S(1)}, f32[1]{0:T(128)}, s32[]{:T(128)}, /*index=5*/f32[2,1,256,256]{3,2...) while((s32[]{:T(128)}, f32[1,256,256]{2,1,0:T(8,128)S(1)}, ...), condition=%wide.region_6.7_spmd.clone, body=%wide.region_0.6_spmd.clone.sunk | while | flops 641046528 | bytes 6349332 | solution.py:113
  15.7 1.8 fusion.223
  28.0 1.8 fusion.223
  45.4 9.9 %all-reduce.8 = (f32[4]{0:T(128)S(1)}, f32[4]{0:T(128)S(1)}, f32[4]{0:T(128)S(1)}, f32[4]{0:T(128)S(1)}) all-reduce(f32[4]{0:T(128)S(1)} %dynamic-update-slice, f32[4]{0:T(128)S(1)} %fusion.156, f32[4]{0:T(128)S(1)} %dynamic-update-slice.3, f32[4]{0:T(128)S(1)} %dynamic-update-slice.6), channel_id=1, replica_groups=mesh['sp_0'=4,'sp_1'=4,'tp'=16] {'sp_1'}, use_global_device_ids=true, to_apply=%add | all-reduce | flops 16 | bytes 128
  56.0 2.5 fusion.152
  72.9 2.0 fusion.70
  75.6 1.9 fusion.188
  83.3 9.6 %all-reduce.9 = (f32[4]{0:T(128)S(1)}, f32[4]{0:T(128)S(1)}, f32[4]{0:T(128)S(1)}, f32[4]{0:T(128)S(1)}) all-reduce(f32[4]{0:T(128)S(1)} %dynamic-update-slice.1, f32[4]{0:T(128)S(1)} %dynamic-update-slice.4, f32[4]{0:T(128)S(1)} %dynamic-update-slice.5, f32[4]{0:T(128)S(1)} %dynamic-update-slice.7), channel_id=2, replica_groups=mesh['sp_0'=4,'sp_1'=4,'tp'=16] {'sp_0'}, use_global_device_ids=true, to_apply=%add.1 | all-reduce | flops 16 | bytes 128
  121.8 9.5 %all-gather.8 = f32[4,1,256]{2,1,0:T(1,128)S(1)} all-gather(f32[1,1,256]{2,1,0:T(1,128)S(1)} %bitcast.325), channel_id=9, replica_groups=mesh['sp_0'=4,'sp_1'=4,'tp'=16] {'sp_1'}, dimensions={0}, use_global_device_ids=true | all-gather | bytes 5120 | tf_op jit(solution)/shard_map/all_gather | solution.py:32
  131.4 7.0 %all_gather.81 = f32[4,1,256]{2,1,0:T(1,128)S(1)} all-gather(f32[1,1,256]{2,1,0:T(1,128)S(1)} %get-tuple-element.176), channel_id=1, replica_groups=mesh['sp_0'=4,'sp_1'=4,'tp'=16] {'sp_0'}, dimensions={0}, use_global_device_ids=true | all-gather | bytes 5120 | tf_op jit(solution)/shard_map/all_gather | solution.py:32
  139.8 2.6 multiply_reduce_fusion.1
  142.4 2.2 convolution_convert_fusion.1
  145.3 59.8 %reduce-scatter.3.cloned.1.call-done = bf16[32,2048]{1,0:T(8,128)(2,1)} async-done(((bf16[512,2048]{1,0:T(8,128)(2,1)}), bf16[32,2048]{1,0:T(8,128)(2,1)}) %reduce-scatter.3.cloned.1.call-update) | async-done | bytes 131088 | tf_op jit(solution)/shard_map/reduce_scatter | solution.py:227
  207.8 15.6 %all_to_all.15 = bf16[16,5,2048]{2,1,0:T(8,128)(2,1)S(1)} all-to-all(bf16[16,5,2048]{2,1,0:T(8,128)(2,1)S(1)} %reshape.900), channel_id=1, replica_groups=mesh['sp_0'=4,'sp_1'=4,'tp'=16] {'sp_0','sp_1'}, dimensions={0} | all-to-all | bytes 655360 | tf_op jit(solution)/shard_map/all_to_all | solution.py:254
  224.3 122.5 %all_to_all.16 = bf16[16,80,2048]{2,1,0:T(8,128)(2,1)S(1)} all-to-all(bf16[16,80,2048]{2,1,0:T(8,128)(2,1)S(1)} %stack.3), channel_id=1, replica_groups=mesh['sp_0'=4,'sp_1'=4,'tp'=16] {'tp'}, dimensions={0} | all-to-all | bytes 10485760 | tf_op jit(solution)/shard_map/all_to_all | solution.py:16
  346.8 2.3 copy-done.6
  349.2 2.6 fusion.56
  351.8 10.6 %convolution_convert_fusion = bf16[1280,2048]{1,0:T(8,128)(2,1)} fusion(bf16[1280,2048]{1,0:T(8,128)(2,1)} %bitcast.315, f32[1280,256]{1,0:T(8,128)} %fusion.56, bf16[1,256,2048]{2,1,0:T(8,128)(2,1)S(1)} %copy-done, bf16[1,2048,256]{2,1,0:T(8,128)(2,1)S(1)} %copy-done.16), kind=kOutput, calls=%fused_computation.75 | convolution fusion | flops 2688942080 | bytes 13893632 | tf_op jit(solution)/shard_map/dot_general | solution.py:262
  363.1 60.4 %reduce-scatter.5.cloned.1.call-done = bf16[80,2048]{1,0:T(8,128)(2,1)} async-done(((bf16[1280,2048]{1,0:T(8,128)(2,1)}), bf16[80,2048]{1,0:T(8,128)(2,1)}) %reduce-scatter.5.cloned.1.call-update) | async-done | bytes 327696 | tf_op jit(solution)/shard_map/reduce_scatter | solution.py:261
  423.5 1.9 reshape.902
  425.4 7.3 %all-to-all-start.2 = ((bf16[16,5,2048]{2,1,0:T(8,128)(2,1)}), bf16[16,5,2048]{2,1,0:T(8,128)(2,1)S(1)}, u32[]{:S(2)}, u32[]{:S(2)}) async-start(bf16[16,5,2048]{2,1,0:T(8,128)(2,1)} %reshape.902), calls=%async_computation.4 | async-start | bytes 1048576 | tf_op jit(solution)/shard_map/all_to_all | solution.py:268
  432.7 8.7 %all-to-all-done.2 = bf16[16,5,2048]{2,1,0:T(8,128)(2,1)S(1)} async-done(((bf16[16,5,2048]{2,1,0:T(8,128)(2,1)}), bf16[16,5,2048]{2,1,0:T(8,128)(2,1)S(1)}, u32[]{:S(2)}, u32[]{:S(2)}) %all-to-all-start.2) | async-done | bytes 327712 | tf_op jit(solution)/shard_map/all_to_all | solution.py:268
  442.5 1.8 multiply_reduce_fusion
  (170 shorter events, 43.6 us)
Async XLA Ops:
  6.5 345.3 %copy-start = (bf16[1,256,2048]{2,1,0:T(8,128)(2,1)S(1)}, bf16[1,256,2048]{2,1,0:T(8,128)(2,1)}, u32[]{:S(2)}) copy-start(bf16[1,256,2048]{2,1,0:T(8,128)(2,1)} %param.31) | copy-start | bytes 3145732
  6.5 66.4 %all-gather.14.cloned.1.call-start = ((), (), s32[]{:S(2)}) async-start(), calls=%async_computation.8 | async-start | bytes 1310720 | tf_op jit(solution)/shard_map/all_gather | solution.py:32
  10.1 31.5 %copy-start.18 = (u32[256]{0:T(256)S(1)}, u32[256]{0:T(256)}, u32[]{:S(2)}) copy-start(u32[256]{0:T(256)} %constant.127) | copy-start | bytes 3076
  10.1 64.9 %copy-start.17 = (u32[256]{0:T(256)S(1)}, u32[256]{0:T(256)}, u32[]{:S(2)}) copy-start(u32[256]{0:T(256)} %constant.132) | copy-start | bytes 3076
  10.1 10.6 %copy-start.4 = (bf16[2,1,256,256]{3,2,1,0:T(8,128)(2,1)S(1)}, bf16[2,1,256,256]{3,2,1,0:T(8,128)(2,1)}, u32[]{:S(2)}) copy-start(bf16[2,1,256,256]{3,2,1,0:T(8,128)(2,1)} %get-tuple-element.388) | copy-start | bytes 786436 | tf_op jit(solution)/shard_map/vmap()/while
  10.1 10.6 %copy-start.5 = (bf16[2,1,256,256]{3,2,1,0:T(8,128)(2,1)S(1)}, bf16[2,1,256,256]{3,2,1,0:T(8,128)(2,1)}, u32[]{:S(2)}) copy-start(bf16[2,1,256,256]{3,2,1,0:T(8,128)(2,1)} %get-tuple-element.387) | copy-start | bytes 786436 | tf_op jit(solution)/shard_map/vmap()/while
  10.1 11.1 %copy-start.2 = (bf16[2,1,256,256]{3,2,1,0:T(8,128)(2,1)S(1)}, bf16[2,1,256,256]{3,2,1,0:T(8,128)(2,1)}, u32[]{:S(2)}) copy-start(bf16[2,1,256,256]{3,2,1,0:T(8,128)(2,1)} %get-tuple-element.389) | copy-start | bytes 786436 | tf_op jit(solution)/shard_map/vmap()/while
  22.4 10.6 %copy-start.4 = (bf16[2,1,256,256]{3,2,1,0:T(8,128)(2,1)S(1)}, bf16[2,1,256,256]{3,2,1,0:T(8,128)(2,1)}, u32[]{:S(2)}) copy-start(bf16[2,1,256,256]{3,2,1,0:T(8,128)(2,1)} %get-tuple-element.388) | copy-start | bytes 786436 | tf_op jit(solution)/shard_map/vmap()/while
  22.4 10.6 %copy-start.5 = (bf16[2,1,256,256]{3,2,1,0:T(8,128)(2,1)S(1)}, bf16[2,1,256,256]{3,2,1,0:T(8,128)(2,1)}, u32[]{:S(2)}) copy-start(bf16[2,1,256,256]{3,2,1,0:T(8,128)(2,1)} %get-tuple-element.387) | copy-start | bytes 786436 | tf_op jit(solution)/shard_map/vmap()/while
  22.4 11.1 %copy-start.2 = (bf16[2,1,256,256]{3,2,1,0:T(8,128)(2,1)S(1)}, bf16[2,1,256,256]{3,2,1,0:T(8,128)(2,1)}, u32[]{:S(2)}) copy-start(bf16[2,1,256,256]{3,2,1,0:T(8,128)(2,1)} %get-tuple-element.389) | copy-start | bytes 786436 | tf_op jit(solution)/shard_map/vmap()/while
  34.7 103.6 %copy-start.10 = (s32[512]{0:T(512)S(1)}, s32[512]{0:T(512)}, u32[]{:S(2)}) copy-start(s32[512]{0:T(512)} %param.23) | copy-start | bytes 6148
  34.7 104.4 %copy-start.3 = (bf16[2,1,256,256]{3,2,1,0:T(8,128)(2,1)S(1)}, bf16[2,1,256,256]{3,2,1,0:T(8,128)(2,1)}, u32[]{:S(2)}) copy-start(bf16[2,1,256,256]{3,2,1,0:T(8,128)(2,1)} %get-tuple-element.403) | copy-start | bytes 786436
  35.5 104.3 %all-gather.12.cloned.1.call-start = ((), (), s32[]{:S(2)}) async-start(), calls=%async_computation.5 | async-start | bytes 1310720 | tf_op jit(solution)/shard_map/all_gather | solution.py:32
  75.0 130.1 %reduce-scatter.3.cloned.1.call-start = ((), (), s32[]{:S(2)}) async-start(), calls=%async_computation.6 | async-start | bytes 2228224 | tf_op jit(solution)/shard_map/reduce_scatter | solution.py:227
  139.8 2.6 copy-start.9
  139.8 2.6 copy-start.14
  142.4 62.7 %copy-start.7 = (bf16[32,2048]{1,0:T(8,128)(2,1)S(1)}, bf16[32,2048]{1,0:T(8,128)(2,1)}, u32[]{:S(2)}) copy-start(bf16[32,2048]{1,0:T(8,128)(2,1)} %param.17) | copy-start | bytes 393220
  144.6 61.6 %copy-start.12 = (f32[2048]{0:T(1024)S(1)}, f32[2048]{0:T(1024)}, u32[]{:S(2)}) copy-start(f32[2048]{0:T(1024)} %param.26) | copy-start | bytes 24580
  144.6 278.9 %reduce-scatter.5.cloned.1.call-start = ((), (), s32[]{:S(2)}) async-start(), calls=%async_computation.7 | async-start | bytes 5570560 | tf_op jit(solution)/shard_map/reduce_scatter | solution.py:261
  224.3 124.9 %copy-start.15 = (bf16[1,2048,256]{2,1,0:T(8,128)(2,1)S(1)}, bf16[1,2048,256]{2,1,0:T(8,128)(2,1)}, u32[]{:S(2)}) copy-start(bf16[1,2048,256]{2,1,0:T(8,128)(2,1)} %param.29) | copy-start | bytes 3145732
  346.8 2.3 copy-start.6
  349.2 2.6 copy-start.16
  425.4 16.0 %all-to-all-start.2 = ((bf16[16,5,2048]{2,1,0:T(8,128)(2,1)}), bf16[16,5,2048]{2,1,0:T(8,128)(2,1)S(1)}, u32[]{:S(2)}, u32[]{:S(2)}) async-start(bf16[16,5,2048]{2,1,0:T(8,128)(2,1)} %reshape.902), calls=%async_computation.4 | async-start | bytes 1048576 | tf_op jit(solution)/shard_map/all_to_all | solution.py:268
  432.7 11.6 %copy-start.8 = (bf16[32,2048]{1,0:T(8,128)(2,1)S(1)}, bf16[32,2048]{1,0:T(8,128)(2,1)}, u32[]{:S(2)}) copy-start(bf16[32,2048]{1,0:T(8,128)(2,1)} %reduce-scatter.3.cloned.1.call-done) | copy-start | bytes 393220
  (3 other events, 3.7 us)
Sparse Core Ops, SparseCore 0:
  35.6 28.4 all-gather.13
  75.1 28.0 all-gather.11
  144.8 60.2 reduce-scatter.2
  362.5 60.9 reduce-scatter.4
